TPU v7x, 32 devices: a whole 2x2x4 slice. The times are simulated.
32 devices in a mesh: kv: 8 (over z, y), tp: 4 (over x, core).
Axes of the slice: x: 2, y: 2, z: 4, core: 2. Of those that a mesh axis runs over, the one named last changes fastest.
Arguments:
- tokens: bfloat16 [32, 4096], P(None, 'kv'), may hold values from -40 to 40, as said below
- norm_gain: float32 [4096], P('kv'), may hold values from 0.1 to 1.9
- w_query: bfloat16 [4096, 2048], P('kv', 'tp'), may hold values from -0.09375 to 0.09375
- w_key: bfloat16 [4096, 512], P('kv', 'tp'), may hold values from -0.09375 to 0.09375
- w_value: bfloat16 [4096, 512], P('kv', 'tp'), may hold values from -0.09375 to 0.09375
- forget_weight: bfloat16 [4096, 32], replicated, may hold values from -0.09375 to 0.09375
- forget_bias: float32 [32], P('tp'), may hold values from -1 to 3
- kv_cache: bfloat16 [32, 10240, 8, 128], P(None, 'kv', 'tp'), may hold values from -6 to 6
- cum_gates: float32 [32, 32, 10240], P(None, 'tp', 'kv'), may hold values from -10500 to 0, as said below
- lengths: int32 [32], replicated, may hold values from 1 to 10240, as said below
- w_out: bfloat16 [2048, 4096], P('tp', 'kv'), may hold values from -0.25 to 0.25
Outputs:
- mixed: bfloat16 [32, 4096], P(None, 'kv')
- log_weight: float32 [32, 32], P(None, 'tp')
Inputs may be any that keep to these rules, and one draw needn't show every extreme that they name: Columns of tokens come in 16 groups of equal width. `cum_gates`: each row does not rise along the positions. `lengths`: some sequence has all 10240 positions cached.
All inputs are finite; a program needn't handle non-finite values.
Results may differ from a plain program's by a relative error of at most 0.0307.
Values may be sent and summed in bfloat16 or wider, within the bound.
A program may use at most 128 MiB of HBM per device.

v0:
```python
import jax
import jax.numpy as jnp
from jax import lax
from jax.sharding import PartitionSpec as P

norm_eps = 1e-05
masked_floor = -1e30


def finish_rows(row_squares, sum_query, sum_keyval, sum_gate, forget_bias, model_width):
    row_scale = lax.rsqrt(row_squares / model_width + norm_eps)[:, None]
    query = (row_scale * sum_query).astype(jnp.bfloat16)
    keyval = (row_scale * sum_keyval).astype(jnp.bfloat16)
    log_gate = jax.nn.log_sigmoid(row_scale * sum_gate + forget_bias)
    return (query, keyval, log_gate)


def shards(
    tokens,
    norm_gain,
    w_query,
    w_key,
    w_value,
    forget_weight,
    forget_bias,
    kv_cache,
    cum_gates,
    lengths,
    w_out,
):
    rows_count, col_count = tokens.shape
    span_len = kv_cache.shape[1]
    kv_local = kv_cache.shape[2]
    head_size = kv_cache.shape[3] // 2
    heads_local = cum_gates.shape[1]
    group_size = heads_local // kv_local
    model_width = col_count * lax.axis_size("kv")
    tokens_f = tokens.astype(jnp.float32)
    squares = jnp.sum(tokens_f * tokens_f, axis=1)
    normalized_input = (tokens_f * norm_gain).astype(jnp.bfloat16)
    gate_cols = lax.dynamic_slice(
        forget_weight,
        (lax.axis_index("kv") * col_count, lax.axis_index("tp") * heads_local),
        (col_count, heads_local),
    )
    part_query = jnp.dot(normalized_input, w_query, preferred_element_type=jnp.float32)
    part_keyval = jnp.concatenate(
        [
            jnp.dot(normalized_input, w_key, preferred_element_type=jnp.float32),
            jnp.dot(normalized_input, w_value, preferred_element_type=jnp.float32),
        ],
        axis=1,
    )
    part_gate = jnp.dot(normalized_input, gate_cols, preferred_element_type=jnp.float32)
    total_sq, sum_query, sum_keyval, sum_gate = (
        lax.psum(squares.astype(jnp.bfloat16), "kv").astype(jnp.float32),
        lax.psum(part_query.astype(jnp.bfloat16), "kv").astype(jnp.float32),
        lax.psum(part_keyval.astype(jnp.bfloat16), "kv").astype(jnp.float32),
        lax.psum(part_gate.astype(jnp.bfloat16), "kv").astype(jnp.float32),
    )
    query, keyval, log_gate = finish_rows(
        total_sq, sum_query, sum_keyval, sum_gate, forget_bias, model_width
    )
    inv_root = head_size ** (-0.5)
    query_head_rows = query.reshape(rows_count, kv_local, group_size, head_size)
    cached_keys = kv_cache[:, :, :, :head_size]
    cached_vals = kv_cache[:, :, :, head_size:]
    scores = (
        jnp.einsum(
            "bkgd,blkd->bkgl", query_head_rows, cached_keys, preferred_element_type=jnp.float32
        )
        * inv_root
    )
    biased = scores - cum_gates.reshape(rows_count, kv_local, group_size, span_len)
    first_pos = lax.axis_index("kv") * span_len
    positions = first_pos + lax.iota(jnp.int32, span_len)
    in_range = positions[None, :] < lengths[:, None]
    last_pos = lengths - 1
    holds_last = (last_pos >= first_pos) & (last_pos < first_pos + span_len)
    last_index = jnp.clip(last_pos - first_pos, 0, span_len - 1)
    last_cum = jnp.take_along_axis(
        cum_gates, jnp.broadcast_to(last_index[:, None, None], (rows_count, heads_local, 1)), axis=2
    )[:, :, 0]
    cum_query = last_cum + log_gate
    fresh_key_row = keyval[:, : kv_local * head_size].reshape(rows_count, kv_local, head_size)
    value_new = keyval[:, kv_local * head_size :].reshape(rows_count, kv_local, head_size)
    new_biased = (
        jnp.einsum(
            "pnof,pnf->pno", query_head_rows, fresh_key_row, preferred_element_type=jnp.float32
        )
        * inv_root
    )
    new_biased = new_biased - cum_query.reshape(rows_count, kv_local, group_size)
    range_mask = in_range[:, None, None, :]
    owner_mask = holds_last[:, None, None]
    peak_local = jnp.max(jnp.where(range_mask, biased, masked_floor), axis=-1)
    peak_local = jnp.where(owner_mask, jnp.maximum(peak_local, new_biased), peak_local)
    weights = jnp.where(range_mask, jnp.exp(biased - peak_local[..., None]), 0.0)
    new_weight = jnp.where(owner_mask, jnp.exp(new_biased - peak_local), 0.0)
    weight_sum = jnp.sum(weights, axis=-1) + new_weight
    weighted = jnp.einsum(
        "bkgl,blkd->bkgd",
        weights.astype(jnp.bfloat16),
        cached_vals,
        preferred_element_type=jnp.float32,
    )
    weighted = (
        weighted
        + new_weight.astype(jnp.bfloat16).astype(jnp.float32)[..., None]
        * value_new.astype(jnp.float32)[:, :, None, :]
    )
    anchor = jnp.where(holds_last[:, None], cum_query, 0.0).reshape(
        rows_count, kv_local, group_size
    )
    peak = lax.pmax(peak_local, "kv")
    rescale_factor = jnp.exp(peak_local - peak)
    weight_sum, weighted, anchor = lax.psum(
        (weight_sum * rescale_factor, weighted * rescale_factor[..., None], anchor), "kv"
    )
    attended = (
        (weighted / weight_sum[..., None])
        .astype(jnp.bfloat16)
        .reshape(rows_count, heads_local * head_size)
    )
    log_weight = (peak + jnp.log(weight_sum) + anchor).reshape(rows_count, heads_local)
    part_out = jnp.dot(attended, w_out, preferred_element_type=jnp.float32)
    mixed = lax.psum(part_out.astype(jnp.bfloat16), "tp")
    return (mixed, log_weight)


def solution(mesh):
    placed = (
        P(None, "kv"),
        P("kv"),
        P("kv", "tp"),
        P("kv", "tp"),
        P("kv", "tp"),
        P(),
        P("tp"),
        P(None, "kv", "tp", None),
        P(None, "tp", "kv"),
        P(),
        P("tp", "kv"),
    )
    return jax.shard_map(
        shards,
        mesh=mesh,
        in_specs=placed,
        out_specs=(P(None, "kv"), P(None, "tp")),
        check_vma=False,
    )
```

profile of v0, /device:TPU:0, one launch (start us, length us, event | category | flops | bytes accessed | tf_op | source)
XLA Modules:
  0.0 224.6 jit_solution(18268263765218162662)
XLA Ops:
  7.2 0.0 copy-start
  7.2 0.0 all-reduce.4.cloned.1.call-start
  7.2 0.0 copy-start.2
  7.3 41.6 %fusion.40 = (bf16[32,1280,2,64]{3,2,1,0:T(2,128)(2,1)}, bf16[32,1280,2,64]{3,2,1,0:T(2,128)(2,1)}) fusion(bf16[32,1280,2,128]{3,2,1,0:T(2,128)(2,1)} %param.18), kind=kLoop, calls=%fused_computation.64 | loop fusion | bytes 41943040 | tf_op jit(solution)/shard_map/slice | solution.py:66
  48.9 0.0 copy-start.5
  48.9 0.0 copy-start.6
  48.9 1.5 reshape.198
  50.4 0.1 fusion.22
  50.5 0.2 convolution_convert_fusion.1
  50.7 0.1 convolution_convert_fusion.2
  50.9 0.0 copy-done.6
  50.9 0.1 convolution_convert_fusion.3
  51.0 0.8 convolution_convert_fusion.4
  51.8 39.3 %all-reduce.1 = (bf16[32,512]{1,0:T(8,128)(2,1)S(1)}, bf16[32]{0:T(256)(128)(2,1)S(1)}, bf16[32,8]{0,1:T(8,128)(2,1)S(1)}, bf16[32,256]{1,0:T(8,128)(2,1)S(1)}) all-reduce(bf16[32,512]{1,0:T(8,128)(2,1)S(1)} %convolution_convert_fusion.1, bf16[32]{0:T(256)(128)(2,1)S(1)} %fusion.22, ...), channel_id=1, replica_groups=mesh['kv'=8,'tp'=4] {'kv'}, use_global_device_ids=true, to_apply=%region_2.0 | all-reduce | flops 24864 | bytes 99456 | tf_op jit(solution)/shard_map/psum | solution.py:57
  91.2 0.1 multiply_convert_fusion
  91.3 0.1 reshape.197
  91.4 0.1 broadcast_compare_fusion
  91.5 12.1 %select_reduce_fusion = (f32[32,2,4]{2,1,0:T(2,128)S(1)}, f32[32,2,4,1280]{3,2,1,0:T(4,128)S(1)}) fusion(pred[32,1280]{1,0:T(8,128)(4,1)S(1)} %broadcast_compare_fusion, f32[32,2,4,1280]{3,2,1,0:T(4,128)} %reshape.198, bf16[32,2,4,64]{3,2,1,0:T(4,128)(2,1)S(1)} %reshape.197, bf16[32,1280,2,64]{3,2,1,0:T(2,128)(2,1)} %get-tuple-element.15), kind=kOutput, calls=%fused_computation.8 | convolution fusion | flops 43253504 | bytes 13181952 | tf_op jit(solution)/shard_map/bkgd,blkd->bkgl/dot_general | solution.py:69
  103.6 0.1 copy.42
  103.8 0.1 copy.40
  103.9 0.1 reshape.207
  103.9 0.0 copy-start.9
  104.0 2.3 %gather_fusion = f32[256]{0:T(256)S(1)} fusion(f32[32,8,1280]{2,1,0:T(8,128)S(1)} %copy-done.2, s32[256]{0:T(256)S(1)} %reshape.207), kind=kCustom, calls=%fused_computation | custom fusion | bytes 5120 | tf_op jit(solution)/shard_map/jit(take_along_axis)/gather | solution.py:81
  106.2 0.1 gather.7
  106.3 0.1 copy.41
  106.4 0.1 multiply_convert_fusion.1
  106.5 0.1 reshape.218
  106.6 0.2 fusion.41
  106.8 0.1 copy.51
  106.9 0.1 broadcast_select_fusion
  107.0 0.1 copy.44
  107.1 17.1 %pmax.7 = f32[32,2,4]{0,2,1:T(4,128)S(1)} all-reduce(f32[32,2,4]{0,2,1:T(4,128)S(1)} %maximum_select_fusion), channel_id=1, replica_groups=mesh['kv'=8,'tp'=4] {'kv'}, use_global_device_ids=true, to_apply=%region_6.7 | all-reduce | flops 256 | bytes 2048 | tf_op jit(solution)/shard_map/pmax | solution.py:115
  124.2 0.8 fusion.16
  125.0 0.1 copy.48
  125.1 0.1 copy.47
  125.2 0.1 reshape.204
  125.3 0.1 copy.46
  125.4 0.0 copy-start.1
  125.4 10.7 %fusion.13 = f32[32,2,4,64]{3,2,1,0:T(4,128)} fusion(bf16[32,1280,2,64]{3,2,1,0:T(2,128)(2,1)} %get-tuple-element.16, f32[32,2,4,1280]{3,2,1,0:T(4,128)S(1)} %get-tuple-element.21, f32[32,2,4]{2,1,0:T(2,128)S(1)} %copy.44, pred[32,1280]{1,0:T(8,128)(4,1)S(1)} %broadcast_compare_fusion, f32[32,2,4]{2,1,0:T(2,128)S(1)} %copy.47, ...), kind=kOutput, calls=%fused_computation.10 | convolution fusion | flops 42975232 | bytes 11922432 | tf_op jit(solution)/shard_map/bkgl,blkd->bkgd/dot_general | solution.py:101
  136.2 0.0 all-reduce.4.cloned.1.call-update
  136.2 19.6 %all-reduce = (f32[32,2,4]{0,2,1:T(4,128)S(1)}, f32[32,2,4]{0,2,1:T(4,128)S(1)}) all-reduce(f32[32,2,4]{0,2,1:T(4,128)S(1)} %get-tuple-element.10, f32[32,2,4]{0,2,1:T(4,128)S(1)} %bitcast.31), channel_id=1, replica_groups=mesh['kv'=8,'tp'=4] {'kv'}, use_global_device_ids=true, to_apply=%region_9.10 | all-reduce | flops 512 | bytes 4096 | tf_op jit(solution)/shard_map/psum | solution.py:117
  155.8 0.6 add_add_fusion
  156.4 0.1 copy.49
  156.5 49.0 %all-reduce.4.cloned.1.call-done = f32[32,2,4,64]{3,2,1,0:T(4,128)} async-done(((f32[32,2,4,64]{3,2,1,0:T(4,128)}), f32[32,2,4,64]{3,2,1,0:T(4,128)}) %all-reduce.4.cloned.1.call-update) | async-done | bytes 65552 | tf_op jit(solution)/shard_map/psum | solution.py:117
  205.5 1.0 divide_convert_fusion
  206.5 0.1 reshape.201
  206.7 0.2 convolution_convert_fusion
  206.9 10.9 %psum.62 = bf16[32,512]{1,0:T(8,128)(2,1)} all-reduce(bf16[32,512]{1,0:T(8,128)(2,1)S(1)} %convolution_convert_fusion), channel_id=1, replica_groups=mesh['kv'=8,'tp'=4] {'tp'}, use_global_device_ids=true, to_apply=%region_10.11 | all-reduce | flops 16384 | bytes 65536 | tf_op jit(solution)/shard_map/psum | solution.py:127
  (26 shorter events, 0.1 us)
Async XLA Ops:
  7.2 43.3 %copy-start = (bf16[512,512]{1,0:T(8,128)(2,1)S(1)}, bf16[512,512]{1,0:T(8,128)(2,1)}, u32[]{:S(2)}) copy-start(bf16[512,512]{1,0:T(8,128)(2,1)} %param.13) | copy-start | bytes 1572868
  7.2 198.3 %all-reduce.4.cloned.1.call-start = ((), (), s32[]{:S(2)}) async-start(), calls=%async_computation | async-start | bytes 262144 | tf_op jit(solution)/shard_map/psum | solution.py:117
  7.2 41.6 %copy-start.2 = (f32[32,8,1280]{2,1,0:T(8,128)S(1)}, f32[32,8,1280]{2,1,0:T(8,128)}, u32[]{:S(2)}) copy-start(f32[32,8,1280]{2,1,0:T(8,128)} %param.19) | copy-start | bytes 3932164
  48.9 1.5 copy-start.3
  48.9 1.6 copy-start.7
  48.9 1.8 copy-start.5
  48.9 2.0 copy-start.6
  48.9 42.5 %copy-start.8 = (s32[32]{0:T(128)S(1)}, s32[32]{0:T(128)}, u32[]{:S(2)}) copy-start(s32[32]{0:T(128)} %param.20) | copy-start | bytes 388
  103.9 2.9 %copy-start.9 = (f32[8]{0:T(128)S(1)}, f32[8]{0:T(128)}, u32[]{:S(2)}) copy-start(f32[8]{0:T(128)} %param.17) | copy-start | bytes 100
  125.4 81.3 %copy-start.4 = (bf16[512,512]{1,0:T(8,128)(2,1)S(1)}, bf16[512,512]{1,0:T(8,128)(2,1)}, u32[]{:S(2)}) copy-start(bf16[512,512]{1,0:T(8,128)(2,1)} %param.21) | copy-start | bytes 1572868
  125.4 92.3 %copy-start.1 = (bf16[512,512]{1,0:T(8,128)(2,1)S(1)}, bf16[512,512]{1,0:T(8,128)(2,1)}, u32[]{:S(2)}) copy-start(bf16[512,512]{1,0:T(8,128)(2,1)} %param.13) | copy-start | bytes 1572868
Sparse Core Ops, SparseCore 0:
  136.3 69.1 all-reduce.3
where the time goes:
time: 225 us
  blocking collectives  86.9 us (39%)
  waiting for transfers between devices  49 us (22%)
  local copies, waits for them, and re-layouts  46.8 us (21%)
  matrix products  24.5 us (11%)
  between operations  14.3 us (6%)
  other arithmetic  2.95 us (1%)
    psum x1, waiting for transfers between devices, shards(): lax.psum((weight_sum * rescale_factor, weighted * rescale_factor[..., Non...  49 us
    slice x1, local copies, waits for them, and re-layouts, shards(): cached_keys = kv_cache[:, :, :, :head_size]  41.6 us
    psum x1, blocking collectives, shards(): lax.psum(part_query.astype(jnp.bfloat16), 'kv').astype(jnp.float32)  39.3 us
    psum x1, blocking collectives, shards(): lax.psum((weight_sum * rescale_factor, weighted * rescale_factor[..., Non...  19.6 us
    pmax x1, blocking collectives, shards(): peak = lax.pmax(peak_local, 'kv')  17.1 us
    dot_general x1, matrix products, shards(): jnp.einsum('bkgd,blkd->bkgl', query_head_rows, cached_keys, preferred_ele...  12.1 us
    psum x1, blocking collectives, shards(): mixed = lax.psum(part_out.astype(jnp.bfloat16), 'tp')  10.9 us
    dot_general x1, matrix products, shards(): jnp.einsum('bkgl,blkd->bkgd', weights.astype(jnp.bfloat16), cached_vals,...  10.7 us
  transfers between devices with their start and end apart: 1, of which 1 were waited for; matrix products, arithmetic and copies ran while one was open for 0% of the time, Pallas kernels for 0%

commit v1 on v0

--- a/solution.py
+++ b/solution.py
@@ -52,9 +52,10 @@
         axis=1,
     )
     part_gate = jnp.dot(normalized_input, gate_cols, preferred_element_type=jnp.float32)
+    lead_layers_all = lambda message: lax.all_gather(message, "kv").sum(axis=0)
     total_sq, sum_query, sum_keyval, sum_gate = (
         lax.psum(squares.astype(jnp.bfloat16), "kv").astype(jnp.float32),
-        lax.psum(part_query.astype(jnp.bfloat16), "kv").astype(jnp.float32),
+        lead_layers_all(part_query.astype(jnp.bfloat16)).astype(jnp.float32),
         lax.psum(part_keyval.astype(jnp.bfloat16), "kv").astype(jnp.float32),
         lax.psum(part_gate.astype(jnp.bfloat16), "kv").astype(jnp.float32),
     )

time: 225 us -> 256 us (1.14)
  blocking collectives: 86.9 us -> 117 us
    all_gather x0 -> x1, blocking collectives: none -> 30.7 us  [shards(): lead_layers_all = lambda message: lax.all_gather(message, 'kv').sum(axis=0)]
where the time goes in v1:
time: 256 us
  blocking collectives  117 us (46%)
  waiting for transfers between devices  49 us (19%)
  local copies, waits for them, and re-layouts  47 us (18%)
  matrix products  24.4 us (10%)
  between operations  14.3 us (6%)
  other arithmetic  3.73 us (1%)
    psum x1, waiting for transfers between devices, shards(): lax.psum((weight_sum * rescale_factor, weighted * rescale_factor[..., Non...  49 us
    slice x1, local copies, waits for them, and re-layouts, shards(): cached_keys = kv_cache[:, :, :, :head_size]  41.5 us
    psum x1, blocking collectives, shards(): lax.psum(squares.astype(jnp.bfloat16), 'kv').astype(jnp.float32)  38.9 us
    all_gather x1, blocking collectives, shards(): lead_layers_all = lambda message: lax.all_gather(message, 'kv').sum(axis=0)  30.7 us
    psum x1, blocking collectives, shards(): lax.psum((weight_sum * rescale_factor, weighted * rescale_factor[..., Non...  19.6 us
    pmax x1, blocking collectives, shards(): peak = lax.pmax(peak_local, 'kv')  17.1 us
    dot_general x1, matrix products, shards(): jnp.einsum('bkgd,blkd->bkgl', query_head_rows, cached_keys, preferred_ele...  12 us
    psum x1, blocking collectives, shards(): mixed = lax.psum(part_out.astype(jnp.bfloat16), 'tp')  10.9 us
  transfers between devices with their start and end apart: 1, of which 1 were waited for; matrix products, arithmetic and copies ran while one was open for 0% of the time, Pallas kernels for 0%

profile of v1, /device:TPU:0, one launch (start us, length us, event | category | flops | bytes accessed | tf_op | source)
XLA Modules:
  0.0 255.7 jit_solution(2277685316011079738)
XLA Ops:
  7.2 0.0 copy-start
  7.2 0.0 all-reduce.4.cloned.1.call-start
  7.2 0.7 broadcast_compare_fusion.1
  8.0 0.1 copy.40
  8.1 0.1 reshape.213
  8.2 1.8 reshape.203
  10.0 0.0 copy-start.7
  10.0 0.0 copy-start.6
  10.1 2.3 gather_fusion
  12.3 0.1 gather.7
  12.4 0.1 fusion.22
  12.6 0.1 convolution_convert_fusion.2
  12.7 0.1 convolution_convert_fusion.3
  12.9 0.8 convolution_convert_fusion.4
  13.7 0.1 copy.41
  13.8 38.9 %all-reduce.1 = (bf16[32]{0:T(256)(128)(2,1)S(1)}, bf16[32,8]{0,1:T(8,128)(2,1)S(1)}, bf16[32,256]{1,0:T(8,128)(2,1)S(1)}) all-reduce(bf16[32]{0:T(256)(128)(2,1)S(1)} %fusion.22, bf16[32,8]{0,1:T(8,128)(2,1)S(1)} %convolution_convert_fusion.4, bf16[32,256]{1,0:T(8,128)(2,1)S(1)} %pad_maximum_fusion), channel_id=1, replica_groups=mesh['kv'=8,'tp'=4] {'kv'}, use_global_device_ids=true, to_apply=%region_1.0 | all-reduce | flops 8480 | bytes 33920 | tf_op jit(solution)/shard_map/psum | solution.py:57
  52.7 0.1 multiply_convert_fusion.1
  52.7 0.1 reshape.225
  52.8 0.2 convolution_convert_fusion.1
  53.0 30.7 %all-gather = bf16[256,512]{1,0:T(8,128)(2,1)S(1)} all-gather(bf16[32,512]{1,0:T(8,128)(2,1)S(1)} %convolution_convert_fusion.1), channel_id=2, replica_groups=mesh['kv'=8,'tp'=4] {'kv'}, dimensions={0}, use_global_device_ids=true | all-gather | bytes 294912 | tf_op jit(solution)/shard_map/all_gather | solution.py:55
  83.8 0.1 reshape.209
  83.9 0.1 multiply_convert_fusion
  84.1 0.2 fusion.41
  84.3 0.1 copy.51
  84.3 0.1 broadcast_compare_fusion
  84.5 41.5 %fusion.40 = (bf16[32,1280,2,64]{3,2,1,0:T(2,128)(2,1)}, bf16[32,1280,2,64]{3,2,1,0:T(2,128)(2,1)}) fusion(bf16[32,1280,2,128]{3,2,1,0:T(2,128)(2,1)} %param.18), kind=kLoop, calls=%fused_computation.64 | loop fusion | bytes 41943040 | tf_op jit(solution)/shard_map/slice | solution.py:67
  125.9 0.0 copy-start.9
  126.0 12.0 %select_reduce_fusion = (f32[32,2,4]{2,1,0:T(2,128)S(1)}, f32[32,2,4,1280]{3,2,1,0:T(4,128)S(1)}) fusion(pred[32,1280]{1,0:T(8,128)(4,1)S(1)} %broadcast_compare_fusion, f32[32,2,4,1280]{3,2,1,0:T(4,128)S(1)} %reshape.203, bf16[32,2,4,64]{3,2,1,0:T(4,128)(2,1)S(1)} %multiply_convert_fusion, bf16[32,1280,2,64]{3,2,1,0:T(2,128)(2,1)} %get-tuple-element.14), kind=kOutput, calls=%fused_computation.8 | convolution fusion | flops 43253504 | bytes 13181952 | tf_op jit(solution)/shard_map/bkgd,blkd->bkgl/dot_general | solution.py:70
  138.0 0.1 copy.42
  138.1 0.1 broadcast_select_fusion
  138.2 0.1 copy.44
  138.3 17.1 %pmax.7 = f32[32,2,4]{0,2,1:T(4,128)S(1)} all-reduce(f32[32,2,4]{0,2,1:T(4,128)S(1)} %maximum_select_fusion), channel_id=1, replica_groups=mesh['kv'=8,'tp'=4] {'kv'}, use_global_device_ids=true, to_apply=%region_6.7 | all-reduce | flops 256 | bytes 2048 | tf_op jit(solution)/shard_map/pmax | solution.py:116
  155.4 0.8 fusion.16
  156.2 0.1 copy.48
  156.3 0.1 copy.46
  156.4 0.1 copy.47
  156.5 0.1 reshape.210
  156.6 0.0 copy-start.1
  156.6 10.7 %fusion.13 = f32[32,2,4,64]{3,2,1,0:T(4,128)} fusion(bf16[32,1280,2,64]{3,2,1,0:T(2,128)(2,1)} %get-tuple-element.15, f32[32,2,4,1280]{3,2,1,0:T(4,128)S(1)} %get-tuple-element.20, f32[32,2,4]{2,1,0:T(2,128)S(1)} %copy.44, pred[32,1280]{1,0:T(8,128)(4,1)S(1)} %broadcast_compare_fusion, f32[32,2,4]{2,1,0:T(2,128)S(1)} %copy.47, ...), kind=kOutput, calls=%fused_computation.10 | convolution fusion | flops 42975232 | bytes 11922432 | tf_op jit(solution)/shard_map/bkgl,blkd->bkgd/dot_general | solution.py:102
  167.3 0.0 all-reduce.4.cloned.1.call-update
  167.4 19.6 %all-reduce = (f32[32,2,4]{0,2,1:T(4,128)S(1)}, f32[32,2,4]{0,2,1:T(4,128)S(1)}) all-reduce(f32[32,2,4]{0,2,1:T(4,128)S(1)} %get-tuple-element.9, f32[32,2,4]{0,2,1:T(4,128)S(1)} %bitcast.33), channel_id=1, replica_groups=mesh['kv'=8,'tp'=4] {'kv'}, use_global_device_ids=true, to_apply=%region_9.10 | all-reduce | flops 512 | bytes 4096 | tf_op jit(solution)/shard_map/psum | solution.py:118
  186.9 0.6 add_add_fusion
  187.5 0.1 copy.49
  187.6 49.0 %all-reduce.4.cloned.1.call-done = f32[32,2,4,64]{3,2,1,0:T(4,128)} async-done(((f32[32,2,4,64]{3,2,1,0:T(4,128)}), f32[32,2,4,64]{3,2,1,0:T(4,128)}) %all-reduce.4.cloned.1.call-update) | async-done | bytes 65552 | tf_op jit(solution)/shard_map/psum | solution.py:118
  236.6 1.0 divide_convert_fusion
  237.7 0.1 reshape.206
  237.8 0.2 convolution_convert_fusion
  238.0 10.9 %psum.54 = bf16[32,512]{1,0:T(8,128)(2,1)} all-reduce(bf16[32,512]{1,0:T(8,128)(2,1)S(1)} %convolution_convert_fusion), channel_id=1, replica_groups=mesh['kv'=8,'tp'=4] {'tp'}, use_global_device_ids=true, to_apply=%region_10.11 | all-reduce | flops 16384 | bytes 65536 | tf_op jit(solution)/shard_map/psum | solution.py:128
  (28 shorter events, 0.2 us)
Async XLA Ops:
  7.2 45.7 %copy-start = (bf16[512,512]{1,0:T(8,128)(2,1)S(1)}, bf16[512,512]{1,0:T(8,128)(2,1)}, u32[]{:S(2)}) copy-start(bf16[512,512]{1,0:T(8,128)(2,1)} %param.13) | copy-start | bytes 1572868
  7.2 229.4 %all-reduce.4.cloned.1.call-start = ((), (), s32[]{:S(2)}) async-start(), calls=%async_computation | async-start | bytes 262144 | tf_op jit(solution)/shard_map/psum | solution.py:118
  8.2 1.8 copy-start.2
  10.0 2.4 copy-start.3
  10.0 2.5 copy-start.5
  10.0 2.5 copy-start.7
  10.0 2.7 %copy-start.6 = (bf16[512,128]{1,0:T(8,128)(2,1)S(1)}, bf16[512,128]{1,0:T(8,128)(2,1)}, u32[]{:S(2)}) copy-start(bf16[512,128]{1,0:T(8,128)(2,1)} %param.14) | copy-start | bytes 393220
  12.3 72.0 %copy-start.8 = (s32[32]{0:T(128)S(1)}, s32[32]{0:T(128)}, u32[]{:S(2)}) copy-start(s32[32]{0:T(128)} %param.20) | copy-start | bytes 388
  125.9 12.1 %copy-start.9 = (f32[8]{0:T(128)S(1)}, f32[8]{0:T(128)}, u32[]{:S(2)}) copy-start(f32[8]{0:T(128)} %param.17) | copy-start | bytes 100
  156.6 81.2 %copy-start.4 = (bf16[512,512]{1,0:T(8,128)(2,1)S(1)}, bf16[512,512]{1,0:T(8,128)(2,1)}, u32[]{:S(2)}) copy-start(bf16[512,512]{1,0:T(8,128)(2,1)} %param.21) | copy-start | bytes 1572868
  156.6 92.3 %copy-start.1 = (bf16[512,512]{1,0:T(8,128)(2,1)S(1)}, bf16[512,512]{1,0:T(8,128)(2,1)}, u32[]{:S(2)}) copy-start(bf16[512,512]{1,0:T(8,128)(2,1)} %param.13) | copy-start | bytes 1572868
Sparse Core Ops, SparseCore 0:
  167.5 69.1 all-reduce.3
